TPU v7x, 1024 devices: a whole 8x8x8 slice. The times are simulated.
1024 devices in a mesh: dp: 8 (over x), kv: 64 (over z, y), tp: 2 (over core).
Axes of the slice: x: 8, y: 8, z: 8, core: 2. Of those that a mesh axis runs over, the one named last changes fastest.
Arguments:
- tokens: bfloat16 [1024, 4096], P('dp', ('kv', 'tp')), may hold values from -7 to 7
- mix_gain: float32 [4096], replicated, may hold values from 0.1 to 1.9
- query_weight: bfloat16 [16, 128, 4096], P('tp', 'kv'), may hold values from -0.09375 to 0.09375
- forget_weight: bfloat16 [16, 128, 4096], P('tp', 'kv'), may hold values from -0.09375 to 0.09375
- value_weight: bfloat16 [16, 128, 4096], P('tp', 'kv'), may hold values from -0.09375 to 0.09375
- gate_weight: bfloat16 [16, 128, 4096], P('tp', 'kv'), may hold values from -0.09375 to 0.09375
- lower_bound: float32 [16, 128], P('tp'), may hold values from 0.02 to 0.9
- recurrent_state: float32 [1024, 16, 128, 128], P(('dp', 'kv'), 'tp'), may hold values from -3 to 3
- head_gain: float32 [16, 128], P('tp'), may hold values from 0.1 to 1.9
- out_weight: bfloat16 [16, 128, 4096], P(None, None, ('kv', 'tp')), may hold values from -0.125 to 0.125
- mlp_gain: float32 [4096], replicated, may hold values from 0.1 to 1.9
- up_weight: bfloat16 [4096, 16384], P(None, ('kv', 'tp')), may hold values from -0.09375 to 0.09375
- down_weight: bfloat16 [16384, 4096], P(('kv', 'tp')), may hold values from -0.1875 to 0.1875
Outputs:
- layer_output: bfloat16 [1024, 4096], P('dp', ('kv', 'tp'))
- next_state: float32 [1024, 16, 128, 128], P(('dp', 'kv'), 'tp')
All inputs are finite; a program needn't handle non-finite values.
Results may differ from a plain program's by a relative error of at most 0.0072.
Values may be sent and summed in bfloat16 or wider, within the bound.
A program may use at most 32 MiB of HBM per device.

v0:
```python
import jax
import jax.numpy as jnp
from jax import lax
from jax.sharding import Mesh
from jax.sharding import PartitionSpec as P

KV_TP = ("kv_0", "kv_1", "tp")
KV = ("kv_0", "kv_1")
DP_KV = ("dp", "kv_0", "kv_1")


epsilon = 1e-06


def in_one_piece(arrays, axis, split_dim, concat_dim, along):
    ends, at = ([], 0)
    for a in arrays[:-1]:
        at += a.shape[along]
        ends.append(at)
    both = jnp.concatenate(arrays, axis=along)
    return tuple(
        jnp.split(
            lax.all_to_all(both, axis, split_axis=split_dim, concat_axis=concat_dim, tiled=True),
            ends,
            axis=along,
        )
    )


def in_order(tiles, dim):
    tiles = jnp.moveaxis(tiles, 0, dim)
    lengths = tiles.shape
    return tiles.reshape(*lengths[:dim], lengths[dim] * lengths[dim + 1], *lengths[dim + 2 :])


def copy_for_each(array, axis):
    copies = jnp.broadcast_to(array, (lax.axis_size(axis), *array.shape))
    return lax.all_to_all(copies, axis, split_axis=0, concat_axis=0, tiled=True)


def gather_directly(array, axis, dim):
    return in_order(copy_for_each(array, axis), dim)


def own_block(tiles, axes, sequence):
    inside = tiles.shape[1:]
    tiles = tiles.reshape(*(lax.axis_size(a) for a in axes), *inside)
    tiles = jnp.moveaxis(tiles, sequence, range(len(axes))).reshape(-1, *inside)
    for k in sequence:
        tiles = lax.psum_scatter(tiles, axes[k], scatter_dimension=0, tiled=True)
    return tiles[0]


def cut_along(array, dim, size):
    before, after = (array.shape[:dim], array.shape[dim + 1 :])
    return jnp.moveaxis(array.reshape(*before, size, -1, *after), dim, 0)


def summed_rows(array, axes, sequence, dim):
    size = lax.axis_size(axes)
    return own_block(cut_along(array, dim, size), axes, sequence)


def normed_rows(row_block, gain_vector):
    whole_rows = lax.all_gather(row_block, KV_TP, axis=1, tiled=True).astype(jnp.float32)
    inv_root = lax.rsqrt(jnp.mean(whole_rows * whole_rows, axis=1, keepdims=True) + epsilon)
    result_rows = (whole_rows * inv_root * gain_vector).astype(jnp.bfloat16)
    return result_rows


def local(
    tokens,
    mix_gain,
    query_weight,
    forget_weight,
    value_weight,
    gate_weight,
    lower_bound,
    recurrent_state,
    head_gain,
    out_weight,
    mlp_gain,
    up_weight,
    down_weight,
):
    normed = normed_rows(tokens, mix_gain)
    local_heads, local_chan, width = query_weight.shape
    stacked = jnp.stack((query_weight, forget_weight, value_weight, gate_weight), axis=0).reshape(
        -1, width
    )
    product = lax.dot_general(
        normed, stacked, (((1,), (1,)), ((), ())), preferred_element_type=jnp.float32
    ).astype(jnp.bfloat16)
    product = product.reshape(normed.shape[0], 4, local_heads, local_chan)
    pre_query, pre_forget, value_rows, pre_gate = in_one_piece(
        (product[:, 0], product[:, 1], product[:, 2], product[:, 3]), KV, 0, 2, 1
    )
    log_forget = jnp.logaddexp(
        jnp.log(lower_bound),
        jnp.log1p(-lower_bound) + jax.nn.log_sigmoid(pre_forget.astype(jnp.float32)),
    )
    key_rows = -jnp.expm1(log_forget)
    next_state = (
        jnp.exp(log_forget)[:, :, :, None] * recurrent_state
        + key_rows[:, :, :, None] * value_rows.astype(jnp.float32)[:, :, None, :]
    )
    query_act = jax.nn.silu(pre_query.astype(jnp.float32))
    readout = jnp.einsum("bhk,bhkv->bhv", query_act, next_state, precision=lax.Precision.HIGHEST)
    inv_head = lax.rsqrt(jnp.mean(readout * readout, axis=2, keepdims=True) + epsilon)
    mixed_heads = (
        readout * inv_head * head_gain * jax.nn.silu(pre_gate.astype(jnp.float32))
    ).astype(jnp.bfloat16)
    all_heads = gather_directly(mixed_heads, "tp", 1)
    flat_mixed = all_heads.reshape(all_heads.shape[0], -1)
    out_matrix = out_weight.reshape(-1, out_weight.shape[2])
    projected = jnp.dot(
        gather_directly(flat_mixed, KV, 0), out_matrix, preferred_element_type=jnp.float32
    )
    residual = lax.optimization_barrier(
        (tokens.astype(jnp.float32) + projected).astype(jnp.bfloat16)
    )
    normed_mlp = normed_rows(residual, mlp_gain)
    hidden = jnp.square(
        jax.nn.relu(jnp.dot(normed_mlp, up_weight, preferred_element_type=jnp.float32))
    ).astype(jnp.bfloat16)
    summed = summed_rows(
        jnp.dot(hidden, down_weight, preferred_element_type=jnp.float32), KV_TP, (2, 0, 1), 1
    )
    layer_output = (residual.astype(jnp.float32) + summed).astype(jnp.bfloat16)
    return (layer_output, next_state)


def solution(mesh):
    torus = Mesh(
        mesh.devices.reshape(mesh.shape["dp"], 8, 8, mesh.shape["tp"]), ("dp", "kv_0", "kv_1", "tp")
    )
    return jax.shard_map(
        local,
        mesh=torus,
        in_specs=(
            P("dp", KV_TP),
            P(),
            P("tp", KV, None),
            P("tp", KV, None),
            P("tp", KV, None),
            P("tp", KV, None),
            P("tp", None),
            P(DP_KV, "tp", None, None),
            P("tp", None),
            P(None, None, KV_TP),
            P(),
            P(None, KV_TP),
            P(KV_TP, None),
        ),
        out_specs=(P("dp", KV_TP), P(DP_KV, "tp", None, None)),
        check_vma=False,
    )
```

profile of v0, /device:TPU:1, one launch (start us, length us, event | category | flops | bytes accessed | tf_op | source)
XLA Modules:
  0.0 366.5 jit_solution(7202375304856923578)
XLA Ops:
  7.2 0.7 all-gather.3.cloned.1.call-update
  7.9 2.1 pad_maximum_fusion
  10.0 0.2 reshape.57
  10.2 100.7 %all-gather.3.cloned.1.call-done = bf16[128,4096]{0,1:T(8,128)(2,1)} async-done(((bf16[128,32]{0,1:T(8,128)(2,1)}), bf16[128,4096]{0,1:T(8,128)(2,1)}) %all-gather.3.cloned.1.call-update) | async-done | bytes 1048592 | tf_op jit(solution)/shard_map/all_gather | solution.py:65
  110.9 1.8 fusion
  112.7 2.0 convolution_convert_fusion
  114.8 0.8 copy.53
  115.5 7.5 %all-to-all-start = ((bf16[128,32,2]{1,2,0:T(2,128)(2,1)}), bf16[128,32,2]{1,2,0:T(2,128)(2,1)S(1)}, u32[]{:S(2)}, u32[]{:S(2)}) async-start(bf16[128,32,2]{1,2,0:T(2,128)(2,1)} %copy.53), calls=%async_computation | async-start | bytes 131072 | tf_op jit(solution)/shard_map/all_to_all | solution.py:23
  123.1 11.0 %all-to-all-done = bf16[128,32,2]{1,2,0:T(2,128)(2,1)S(1)} async-done(((bf16[128,32,2]{1,2,0:T(2,128)(2,1)}), bf16[128,32,2]{1,2,0:T(2,128)(2,1)S(1)}, u32[]{:S(2)}, u32[]{:S(2)}) %all-to-all-start) | async-done | bytes 16416 | tf_op jit(solution)/shard_map/all_to_all | solution.py:23
  134.8 0.6 multiply_add_fusion
  135.5 0.9 copy-done.1
  136.4 1.0 fusion.38
  137.6 5.1 %all_to_all.28 = bf16[2,2,8,128]{3,2,1,0:T(8,128)(2,1)S(1)} all-to-all(bf16[2,2,8,128]{3,2,1,0:T(8,128)(2,1)S(1)} %broadcast_in_dim.4), channel_id=1, replica_groups=mesh['dp'=8,'kv_0'=8,'kv_1'=8,'tp'=2] {'tp'}, dimensions={0} | all-to-all | bytes 16384 | tf_op jit(solution)/shard_map/all_to_all | solution.py:38
  142.7 0.3 broadcast_in_dim.5
  143.0 21.8 %all_to_all.29 = bf16[64,2,2048]{2,1,0:T(2,128)(2,1)S(1)} all-to-all(bf16[64,2,2048]{2,1,0:T(2,128)(2,1)S(1)} %broadcast_in_dim.5), channel_id=1, replica_groups=mesh['dp'=8,'kv_0'=8,'kv_1'=8,'tp'=2] {'kv_0','kv_1'}, dimensions={0} | all-to-all | bytes 1048576 | tf_op jit(solution)/shard_map/all_to_all | solution.py:38
  165.0 0.9 fusion.9
  165.9 81.4 %all-gather.5.cloned.1.call-done = bf16[128,4096]{0,1:T(8,128)(2,1)} async-done(((bf16[128,32]{0,1:T(8,128)(2,1)}), bf16[128,4096]{0,1:T(8,128)(2,1)}) %all-gather.5.cloned.1.call-update) | async-done | bytes 1048592 | tf_op jit(solution)/shard_map/all_gather | solution.py:65
  247.4 1.8 fusion.3
  249.2 3.0 fusion.8
  252.2 1.6 copy.63
  253.9 18.3 %reduce-scatter.4.cloned.1.call-done = f32[64,128,32]{1,2,0:T(8,128)} async-done(((f32[128,128,32]{1,2,0:T(8,128)}), f32[64,128,32]{1,2,0:T(8,128)}) %reduce-scatter.4.cloned.1.call-update) | async-done | bytes 1048592 | tf_op jit(solution)/shard_map/reduce_scatter | solution.py:50
  272.2 44.6 %reduce-scatter.6.cloned.1.call-done = f32[8,128,32]{1,2,0:T(8,128)} async-done(((f32[64,128,32]{1,2,0:T(8,128)}), f32[8,128,32]{1,2,0:T(8,128)}) %reduce-scatter.6.cloned.1.call-update) | async-done | bytes 131088 | tf_op jit(solution)/shard_map/reduce_scatter | solution.py:50
  316.9 41.8 %reduce-scatter.8.cloned.1.call-done = f32[1,128,32]{1,2,0:T(8,128)} async-done(((f32[8,128,32]{1,2,0:T(8,128)}), f32[1,128,32]{1,2,0:T(8,128)}) %reduce-scatter.8.cloned.1.call-update) | async-done | bytes 16400 | tf_op jit(solution)/shard_map/reduce_scatter | solution.py:50
  358.7 1.3 fusion.22
  (52 shorter events, 1.4 us)
Async XLA Ops:
  7.2 242.0 %copy-start = (bf16[128,4096]{1,0:T(8,128)(2,1)S(1)}, bf16[128,4096]{1,0:T(8,128)(2,1)}, u32[]{:S(2)}) copy-start(bf16[128,4096]{1,0:T(8,128)(2,1)} %param.25) | copy-start | bytes 3145732
  7.2 105.5 %copy-start.9 = (f32[4096]{0:T(1024)S(1)}, f32[4096]{0:T(1024)}, u32[]{:S(2)}) copy-start(f32[4096]{0:T(1024)} %param.14) | copy-start | bytes 49156
  7.2 103.7 %all-gather.3.cloned.1.call-start = ((), (), s32[]{:S(2)}) async-start(), calls=%async_computation.6 | async-start | bytes 1056768 | tf_op jit(solution)/shard_map/all_gather | solution.py:65
  10.0 113.1 %copy-start.7 = (f32[8,128]{1,0:T(8,128)S(1)}, f32[8,128]{1,0:T(8,128)}, u32[]{:S(2)}) copy-start(f32[8,128]{1,0:T(8,128)} %param.19) | copy-start | bytes 12292
  10.2 124.6 %copy-start.2 = (f32[2,8,128,128]{3,2,1,0:T(8,128)S(1)}, f32[2,8,128,128]{3,2,1,0:T(8,128)}, u32[]{:S(2)}) copy-start(f32[2,8,128,128]{3,2,1,0:T(8,128)} %param.20) | copy-start | bytes 3145732
  115.5 18.6 %all-to-all-start = ((bf16[128,32,2]{1,2,0:T(2,128)(2,1)}), bf16[128,32,2]{1,2,0:T(2,128)(2,1)S(1)}, u32[]{:S(2)}, u32[]{:S(2)}) async-start(bf16[128,32,2]{1,2,0:T(2,128)(2,1)} %copy.53), calls=%async_computation | async-start | bytes 131072 | tf_op jit(solution)/shard_map/all_to_all | solution.py:23
  123.1 124.3 %all-gather.5.cloned.1.call-start = ((), (), s32[]{:S(2)}) async-start(), calls=%async_computation.7 | async-start | bytes 1056768 | tf_op jit(solution)/shard_map/all_gather | solution.py:65
  134.2 3.3 copy-start.8
  135.4 1.0 copy-start.1
  135.5 29.5 %copy-start.3 = (bf16[16,128,32]{1,2,0:T(8,128)(2,1)S(1)}, bf16[16,128,32]{1,2,0:T(8,128)(2,1)}, u32[]{:S(2)}) copy-start(bf16[16,128,32]{1,2,0:T(8,128)(2,1)} %param.22) | copy-start | bytes 393220
  135.5 29.5 %copy-start.5 = (bf16[128,32]{0,1:T(8,128)(2,1)S(1)}, bf16[128,32]{0,1:T(8,128)(2,1)}, u32[]{:S(2)}) copy-start(bf16[128,32]{0,1:T(8,128)(2,1)} %param.13) | copy-start | bytes 24580
  142.7 106.5 %copy-start.6 = (f32[4096]{0:T(1024)S(1)}, f32[4096]{0:T(1024)}, u32[]{:S(2)}) copy-start(f32[4096]{0:T(1024)} %param.23) | copy-start | bytes 49156
  165.9 106.3 %reduce-scatter.4.cloned.1.call-start = ((), (), s32[]{:S(2)}) async-start(), calls=%async_computation.8 | async-start | bytes 3145728 | tf_op jit(solution)/shard_map/reduce_scatter | solution.py:50
  253.8 104.9 %copy-start.4 = (bf16[128,32]{0,1:T(8,128)(2,1)S(1)}, bf16[128,32]{0,1:T(8,128)(2,1)}, u32[]{:S(2)}) copy-start(bf16[128,32]{0,1:T(8,128)(2,1)} %fusion.9) | copy-start | bytes 24580
  253.8 63.0 %reduce-scatter.6.cloned.1.call-start = ((), (), s32[]{:S(2)}) async-start(), calls=%async_computation.9 | async-start | bytes 1179648 | tf_op jit(solution)/shard_map/reduce_scatter | solution.py:50
  272.2 86.4 %reduce-scatter.8.cloned.1.call-start = ((), (), s32[]{:S(2)}) async-start(), calls=%async_computation.10 | async-start | bytes 147456 | tf_op jit(solution)/shard_map/reduce_scatter | solution.py:50
Sparse Core Ops, SparseCore 0:
  12.2 98.6 all-gather.2
  166.0 81.3 all-gather.4
  253.9 18.2 reduce-scatter.3
  275.4 41.3 reduce-scatter.5
  320.0 38.5 reduce-scatter.7
where the time goes:
time: 372 us; the launch traced here: 367 us
  waiting for transfers between devices  299 us (80%)
  blocking collectives  26.9 us (7%)
  between operations  14 us (4%)
  other arithmetic  7.85 us (2%)
  starting transfers between devices  7.74 us (2%)
  matrix products  6.9 us (2%)
  local copies, waits for them, and re-layouts  4.55 us (1%)
    all_gather x2, waiting for transfers between devices, normed_rows(): lax.all_gather(row_block, KV_TP, axis=1, tiled=True).astype(jnp.float32)  182 us
    reduce_scatter x3, waiting for transfers between devices, own_block(): tiles = lax.psum_scatter(tiles, axes[k], scatter_dimension=0, tiled=True)  105 us
    all_to_all x2, blocking collectives, copy_for_each(): return lax.all_to_all(copies, axis, split_axis=0, concat_axis=0, tiled=True)  26.9 us
    all_to_all x1, waiting for transfers between devices, in_one_piece(): lax.all_to_all(both, axis, split_axis=split_dim, concat_axis=concat_dim,...  11 us
    all_to_all x1, starting transfers between devices, in_one_piece(): lax.all_to_all(both, axis, split_axis=split_dim, concat_axis=concat_dim,...  7.54 us
  transfers between devices with their start and end apart: 6, of which 6 were waited for; matrix products, arithmetic and copies ran while one was open for 1% of the time, Pallas kernels for 0%

commit v1 on v0

v1 whole, which is shorter than its diff:
```python
import jax
import jax.numpy as jnp
from jax import lax
from jax.experimental import pallas as pl
from jax.experimental.pallas import tpu as pltpu
from jax.sharding import Mesh
from jax.sharding import PartitionSpec as P

KV_TP = ("kv_0", "kv_1", "tp")
KV = ("kv_0", "kv_1")
DP_KV = ("dp", "kv_0", "kv_1")
MESH = pl.DeviceIdType.MESH
F32 = jnp.float32
BF16 = jnp.bfloat16
EPS = 1e-06
FAR = (4, 3, 5, 2, 6, 1, 7)
NEAR = (1, 7, 2, 6, 3, 5, 4)


class Place:
    def __init__(self):
        self.x, self.z, self.y, self.tp = (lax.axis_index(n) for n in ("dp", "kv_0", "kv_1", "tp"))
        self.other = 1 - self.tp
        self.partner = (self.x, self.z, self.y, self.other)
        self.a = self.y * self.other + self.z * self.tp
        self.b = self.z * self.other + self.y * self.tp

    def device(self, d, e):
        z = lax.rem(self.z + d * self.tp + e * self.other, 8)
        y = lax.rem(self.y + d * self.other + e * self.tp, 8)
        return (self.x, z, y, self.tp)

    def kv(self, d, e):
        _, z, y, _ = self.device(d, e)
        return z * 8 + y

    def ab(self, d, e):
        return lax.rem(self.a + d, 8), lax.rem(self.b + e, 8)


def kv_of(tp, a, b):
    return (1 - tp) * (b * 8 + a) + tp * (a * 8 + b)


def remote(src, dst, send, recv, device):
    return pltpu.make_async_remote_copy(src, dst, send, recv, device_id=device, device_id_type=MESH)


def landed(ref, sem):
    pltpu.make_async_copy(ref, ref, sem).wait()


def dot(a, b, ca, cb):
    return lax.dot_general(a, b, (((ca,), (cb,)), ((), ())), preferred_element_type=F32)


def gather_first(me, own, block, sems):
    sa, ra, sb, rb = sems
    for d in FAR:
        remote(own, block(0, 0), sa, ra.at[d], me.device(d, 0)).start()
    for e in FAR:
        remote(own, block(0, 0), sb, rb.at[e], me.device(0, e)).start()


def gather_second(me, own, block, sems):
    sa, ra, sb, rb = sems
    for d in NEAR:
        landed(own, ra.at[d])
        for e in FAR:
            remote(block(d, 0), block(d, 0), sb, rb.at[e], me.device(0, e)).start()


def gather_drain(own, row, sems):
    sa, ra, sb, rb = sems
    for _ in range(7):
        landed(own, sa)
        landed(row, sb)


def column_mask(shape, lo, hi):
    lane = lax.broadcasted_iota(jnp.int32, shape, 1)
    return (lane >= lo) & (lane < hi)


def squeezed_lanes(tile_of, tp, b, half):
    result = None
    for i in range(4):
        kv = kv_of(tp, half * 4 + i, b)
        tile, off = kv // 2, lax.rem(kv, 2) * 64 + tp * 32
        v = pltpu.roll(tile_of(tile), lax.rem(i * 32 + 128 - off, 128), 1)
        result = v if result is None else jnp.where(column_mask(v.shape, i * 32, i * 32 + 32), v, result)
    return result


def kernel(
    x_h, mg_h, q_h, f_h, v_h, g_h, lb_h, st_h, hg_h, ow_h, lg_h, up_h, dn_h,
    out_ref, nst_h,
    xv, mg, lg, lb, hg, wraw, upr, dnr, owr, st, nst,
    X, R, D, W2o, W2p, UTs, UTp, DTs, DTp, OWp,
    px1, pr1, px2, pr2, px3, pr3,
    tr, S, B, lbs, msk, O, msg, res, Y, R1, T, R2, wt,
    hs, sa1, ra1, sb1, rb1, sa2, ra2, sb2, rb2, sa3, ra3, sb3, rb3,
    s_a2a, r_a2a, s1, r1, s2, r2, sd, rd, so,
):
    me = Place()
    tp, other = me.tp, me.other

    bar = pltpu.get_barrier_semaphore()
    for d in range(1, 8):
        pl.semaphore_signal(bar, inc=1, device_id=me.device(d, 0), device_id_type=MESH)
        pl.semaphore_signal(bar, inc=1, device_id=me.device(0, d), device_id_type=MESH)
    pl.semaphore_signal(bar, inc=1, device_id=me.partner, device_id_type=MESH)

    loads = []

    def load(src, dst, k):
        cp = pltpu.make_async_copy(src, dst, hs.at[k])
        cp.start()
        return cp

    l_x = load(x_h, xv, 0)
    l_mg = load(mg_h, mg, 1)
    for kind, w in enumerate((q_h, f_h, v_h, g_h)):
        for h in range(8):
            pltpu.make_async_copy(w.at[h], wraw.at[pl.ds(kind * 16 + h * 2, 2)], hs.at[2]).start()
    l_lg = load(lg_h, lg, 3)
    l_lb = load(lb_h, lb, 4)
    l_hg = load(hg_h, hg, 5)
    l_ow = load(ow_h, owr, 6)
    l_st = load(st_h, st, 7)
    l_up = load(up_h, upr, 8)
    l_dn = load(dn_h, dnr, 9)

    l_mg.wait()
    landed(wraw, hs.at[2])

    def prep_w(i, _):
        b, half = i // 2, lax.rem(i, 2)

        def tile_of(t):
            w = wraw[:, pl.ds(pl.multiple_of(t * 128, 128), 128)].astype(F32)
            return w * mg[pl.ds(t, 1), :]

        W2o[b, half] = squeezed_lanes(tile_of, tp, b, half).astype(BF16)
        wt[b, half] = squeezed_lanes(tile_of, other, b, half).astype(BF16)
        return 0

    lax.fori_loop(0, 16, prep_w, 0)
    l_x.wait()
    l_ow.wait()

    pl.semaphore_wait(bar, 15)

    def x_block(d, e):
        a, b = me.ab(8 - d, 8 - e)
        return X.at[b, a]

    sems1 = (sa1, ra1, sb1, rb1)
    gather_first(me, xv, x_block, sems1)
    X[me.b, me.a] = xv[...]
    remote(wt, W2p, sd.at[0], rd.at[0], me.partner).start()
    remote(owr.at[pl.ds(other * 8, 8)], OWp, sd.at[1], rd.at[1], me.partner).start()
    gather_second(me, xv, x_block, sems1)

    landed(W2p, rd.at[0])

    def mm1(e, acc, sq):
        b = lax.rem(me.b + 8 - e, 8)
        xr = X[b].reshape(256, 128)
        xf = xr.astype(F32)
        sq = sq + jnp.sum(xf * xf, axis=0, keepdims=True)
        for half in range(2):
            w = jnp.concatenate([W2o[b, half], W2p[b, half]], axis=0)
            acc = acc + dot(w, xr[half * 128 : half * 128 + 128], 1, 0)
        return acc, sq

    acc, sq = jnp.zeros((128, 128), F32), jnp.zeros((1, 128), F32)
    for e in (0,) + NEAR:
        if e:
            landed(X.at[0], rb1.at[e])
        acc, sq = mm1(e, acc, sq)
    px1[0:64] = acc[64:128]
    px1[64:72] = jnp.broadcast_to(sq, (8, 128))
    remote(px1, pr1, sd.at[2], rd.at[2], me.partner).start()
    landed(pr1, rd.at[2])
    inv = lax.rsqrt((sq + pr1[64:65]) * (1.0 / 4096.0) + EPS)
    pre = ((acc[0:64] + pr1[0:64]) * inv).astype(BF16).astype(F32)
    tr[...] = pre.T
    S[...] = jnp.concatenate([tr[pl.ds(0, 64, stride=2), :], tr[pl.ds(1, 64, stride=2), :]], axis=1)

    mine = me.kv(0, 0)
    order = sorted(
        ((d, e) for d in range(8) for e in range(8) if d or e),
        key=lambda t: -(min(t[0], 8 - t[0]) + min(t[1], 8 - t[1])),
    )
    for d, e in order:
        k = me.kv(d, e)
        remote(S.at[pl.ds(k, 1)], B.at[pl.ds(mine, 1)], s_a2a, r_a2a, me.device(d, e)).start()
    B[pl.ds(mine, 1), :] = S[pl.ds(mine, 1), :]

    l_lb.wait()
    lane = lax.broadcasted_iota(jnp.int32, (8, 128), 1)
    head = lax.broadcasted_iota(jnp.int32, (8, 128), 0)
    sel = (lax.rem(lane, 64) // 2 == 8 + head).astype(F32)
    lbs[...] = lax.dot_general(
        lb[...], sel, (((0,), (0,)), ((), ())), precision=lax.Precision.HIGHEST, preferred_element_type=F32
    )
    odd = lax.rem(lax.broadcasted_iota(jnp.int32, (64, 128), 1), 2)
    low = jnp.where(odd == 0, lbs[pl.ds(0, 64, stride=2), :], lbs[pl.ds(1, 64, stride=2), :])
    l_lg.wait()
    l_up.wait()

    def prep_up(i, _):
        b, half = i // 2, lax.rem(i, 2)
        for core in range(2):
            rows = [upr[kv_of(core, half * 4 + j, b), core] for j in range(4)]
            u = jnp.concatenate(rows, axis=0).astype(F32).T
            g = squeezed_lanes(lambda t: lg[pl.ds(t, 1), :], core, b, half)
            UTs[core, b, half] = (u * g).astype(BF16)
        return 0

    lax.fori_loop(0, 16, prep_up, 0)
    remote(UTs.at[other], UTp, sd.at[3], rd.at[3], me.partner).start()

    l_st.wait()
    l_hg.wait()
    landed(B.at[pl.ds(0, 63)], r_a2a)
    Bv = B[...]
    ex = jnp.exp(-jnp.abs(Bv))
    big = 1.0 / (1.0 + ex)
    small = ex * big
    sig = jnp.where(Bv >= 0, big, small)
    sig_neg = jnp.where(Bv >= 0, small, big)
    decay = low + (1.0 - low) * sig
    key = (1.0 - low) * sig_neg
    act = Bv * sig
    Bb = Bv.astype(BF16)
    src = lax.broadcasted_iota(jnp.int32, (64, 128), 0)
    col = lax.broadcasted_iota(jnp.int32, (64, 128), 1)
    zero = jnp.zeros_like(Bb)
    spread = dot(jnp.where(odd == 0, Bb, zero), (col == 2 * src).astype(BF16), 0, 0)
    spread = spread + dot(jnp.where(odd == 1, Bb, zero), (col == 2 * src + 1).astype(BF16), 0, 0)
    msk[...] = spread
    vg = msk[pl.ds(0, 64, stride=2), :] + msk[pl.ds(1, 64, stride=2), :]
    for tok in range(2):
        for h in range(8):
            total = None
            vrow = vg[tok * 32 + 16 + h : tok * 32 + 17 + h]
            for j in range(2):
                c = tok * 64 + 2 * h + j
                old = st[tok, h, pl.ds(j, 64, stride=2), :]
                new = decay[:, c + 16 : c + 17] * old + key[:, c + 16 : c + 17] * vrow
                nst[tok, h, pl.ds(j, 64, stride=2), :] = new
                part = act[:, c : c + 1] * new
                total = part if total is None else total + part
            O[tok, h : h + 1, :] = jnp.sum(total, axis=0, keepdims=True)
    pltpu.make_async_copy(nst, nst_h, so).start()
    mixed = []
    for tok in range(2):
        o = O[tok]
        gate = vg[tok * 32 + 24 : tok * 32 + 32]
        ge = jnp.exp(-jnp.abs(gate))
        gs = jnp.where(gate >= 0, 1.0, ge) / (1.0 + ge)
        inv_head = lax.rsqrt(jnp.mean(o * o, axis=1, keepdims=True) + EPS)
        mixed.append(o * inv_head * hg[...] * (gate * gs))
    msg[...] = jnp.stack(mixed, axis=1).astype(BF16)

    def d_block(d, e):
        return D.at[:, me.kv(8 - d, 8 - e)]

    sems2 = (sa2, ra2, sb2, rb2)
    gather_first(me, msg, d_block, sems2)
    D[:, mine] = msg[...]
    gather_second(me, msg, d_block, sems2)

    l_dn.wait()

    def prep_dn(r, _):
        t = dnr[:, pl.ds(pl.multiple_of(r * 128, 128), 128)].astype(F32).T.astype(BF16)
        DTs[0, 2 * r] = t[0:32]
        DTs[1, 2 * r] = t[32:64]
        DTs[0, 2 * r + 1] = t[64:96]
        DTs[1, 2 * r + 1] = t[96:128]
        return 0

    lax.fori_loop(0, 32, prep_dn, 0)
    remote(DTs.at[other], DTp, sd.at[4], rd.at[4], me.partner).start()

    landed(OWp, rd.at[1])
    for e in NEAR:
        landed(D.at[:, pl.ds(0, 8)], rb2.at[e])
    heads = D.reshape(8, 128, 128)
    acc2 = jnp.zeros((64, 128), F32)
    for h in range(8):
        w = jnp.concatenate([owr[tp * 8 + h], OWp[h]], axis=0)
        acc2 = acc2 + dot(w, heads[h], 1, 1)
    px2[...] = acc2[32:64]
    remote(px2, pr2, sd.at[5], rd.at[5], me.partner).start()
    landed(pr2, rd.at[5])
    res[...] = (xv[...].astype(F32) + acc2[0:32] + pr2[...]).astype(BF16)

    def r_block(d, e):
        a, b = me.ab(8 - d, 8 - e)
        return R.at[b, a]

    sems3 = (sa3, ra3, sb3, rb3)
    gather_first(me, res, r_block, sems3)
    R[me.b, me.a] = res[...]
    gather_second(me, res, r_block, sems3)

    landed(UTp, rd.at[3])

    def mm3(e, acc, sq):
        b = lax.rem(me.b + 8 - e, 8)
        xr = R[b].reshape(256, 128)
        xf = xr.astype(F32)
        sq = sq + jnp.sum(xf * xf, axis=0, keepdims=True)
        for half in range(2):
            w = jnp.concatenate([UTs[tp, b, half], UTp[b, half]], axis=0)
            acc = acc + dot(w, xr[half * 128 : half * 128 + 128], 1, 0)
        return acc, sq

    acc3, sq3 = jnp.zeros((256, 128), F32), jnp.zeros((1, 128), F32)
    for e in (0,) + NEAR:
        if e:
            landed(R.at[0], rb3.at[e])
        acc3, sq3 = mm3(e, acc3, sq3)
    px3[0:256] = acc3
    px3[256:264] = jnp.broadcast_to(sq3, (8, 128))
    remote(px3, pr3, sd.at[6], rd.at[6], me.partner).start()
    landed(pr3, rd.at[6])
    inv3 = lax.rsqrt((sq3 + pr3[256:257]) * (1.0 / 4096.0) + EPS)
    pre3 = jnp.concatenate([acc3[0:128] + pr3[128:256], acc3[128:256] + pr3[0:128]], axis=0)
    act3 = jnp.maximum(pre3 * inv3, 0.0)
    hidden = (act3 * act3).astype(BF16)

    landed(DTp, rd.at[4])
    first = None
    for d in FAR + (0,):
        rows = []
        for e in range(8):
            k = me.kv(d, e)
            rows.append(jnp.concatenate([DTs[tp, k], DTp[k]], axis=1))
        y = dot(jnp.concatenate(rows, axis=0), hidden, 1, 0)
        Y[d, 0] = y[0:32]
        Yb = y.astype(BF16)
        for e in range(1, 8):
            T[d, e] = Yb[e * 32 : e * 32 + 32]
        for e in FAR:
            remote(T.at[d, e], R1.at[d, e], s1, r1.at[d], me.device(0, e)).start()
    for d in FAR + (0,):
        landed(R1.at[0, pl.ds(0, 7)], r1.at[d])
        t = Y[d, 0]
        for e in range(1, 8):
            t = t + R1[d, e].astype(F32)
        if d:
            T[d, 0] = t.astype(BF16)
            remote(T.at[d, 0], R2.at[d], s2, r2.at[d], me.device(d, 0)).start()
        else:
            first = t
    total = res[...].astype(F32) + first
    for d in NEAR:
        landed(R2.at[d], r2.at[d])
        total = total + R2[d].astype(F32)
    out_ref[...] = total.astype(BF16)

    gather_drain(xv, X.at[0], sems1)
    gather_drain(msg, D.at[:, pl.ds(0, 8)], sems2)
    gather_drain(res, R.at[0], sems3)
    landed(B.at[pl.ds(0, 63)], s_a2a)
    for d in range(8):
        landed(R1.at[0, pl.ds(0, 7)], s1)
    landed(R2.at[pl.ds(0, 7)], s2)
    landed(wt, sd.at[0])
    landed(OWp, sd.at[1])
    landed(px1, sd.at[2])
    landed(UTp, sd.at[3])
    landed(DTp, sd.at[4])
    landed(px2, sd.at[5])
    landed(px3, sd.at[6])
    pltpu.make_async_copy(nst, nst_h, so).wait()


def local(tokens, mix_gain, q, f, v, g, lower, state, head_gain, out_w, mlp_gain, up, down):
    dma = pltpu.SemaphoreType.DMA
    gather_sems = [dma, dma((8,)), dma, dma((8,))]
    vm = pltpu.VMEM
    out, nst = pl.pallas_call(
        kernel,
        out_shape=(jax.ShapeDtypeStruct((32, 128), BF16), jax.ShapeDtypeStruct(state.shape, F32)),
        in_specs=[pl.BlockSpec(memory_space=pltpu.HBM)] * 13,
        out_specs=(pl.BlockSpec(memory_space=pltpu.VMEM), pl.BlockSpec(memory_space=pltpu.HBM)),
        scratch_shapes=[
            vm((32, 128), BF16), vm((32, 128), F32), vm((32, 128), F32), vm((8, 128), F32), vm((8, 128), F32),
            vm((64, 4096), BF16), vm((64, 2, 32, 128), BF16), vm((128, 4096), BF16), vm((16, 32, 128), BF16),
            vm((2, 8, 128, 128), F32), vm((2, 8, 128, 128), F32),
            vm((8, 8, 32, 128), BF16), vm((8, 8, 32, 128), BF16), vm((8, 64, 2, 128), BF16),
            vm((8, 2, 64, 128), BF16), vm((8, 2, 64, 128), BF16),
            vm((2, 8, 2, 128, 128), BF16), vm((8, 2, 128, 128), BF16),
            vm((2, 64, 32, 128), BF16), vm((64, 32, 128), BF16), vm((8, 32, 128), BF16),
            vm((72, 128), F32), vm((72, 128), F32), vm((32, 128), F32), vm((32, 128), F32),
            vm((264, 128), F32), vm((264, 128), F32),
            vm((128, 64), F32), vm((64, 128), F32), vm((64, 128), F32), vm((128, 128), F32), vm((128, 128), F32),
            vm((2, 8, 128), F32), vm((8, 2, 128), BF16), vm((32, 128), BF16),
            vm((8, 1, 32, 128), F32), vm((8, 8, 32, 128), BF16), vm((8, 8, 32, 128), BF16), vm((8, 32, 128), BF16),
            vm((8, 2, 64, 128), BF16),
            dma((10,)), *gather_sems, *gather_sems, *gather_sems,
            dma, dma, dma, dma((8,)), dma, dma((8,)), dma((7,)), dma((7,)), dma,
        ],
        compiler_params=pltpu.CompilerParams(collective_id=0, has_side_effects=True, vmem_limit_bytes=60 * 1024 * 1024),
    )(
        tokens.T, mix_gain.reshape(32, 128), q, f, v, g, lower, state, head_gain,
        out_w.transpose(0, 2, 1), mlp_gain.reshape(32, 128), up.reshape(64, 2, 32, 128), down,
    )
    return (out.T, nst)


def solution(mesh):
    torus = Mesh(
        mesh.devices.reshape(mesh.shape["dp"], 8, 8, mesh.shape["tp"]), ("dp", "kv_0", "kv_1", "tp")
    )
    return jax.shard_map(
        local,
        mesh=torus,
        in_specs=(
            P("dp", KV_TP), P(), P("tp", KV, None), P("tp", KV, None), P("tp", KV, None), P("tp", KV, None),
            P("tp", None), P(DP_KV, "tp", None, None), P("tp", None), P(None, None, KV_TP), P(),
            P(None, KV_TP), P(KV_TP, None),
        ),
        out_specs=(P("dp", KV_TP), P(DP_KV, "tp", None, None)),
        check_vma=False,
    )
```

time: 372 us -> 83.5 us (0.22); the launches traced: 367 us -> 82.8 us
  waiting for transfers between devices: 299 us -> 0 us
  Pallas kernels: 0 us -> 78.5 us
  blocking collectives: 26.9 us -> 0 us
  between operations: 14 us -> 0.64 us
  other arithmetic: 7.85 us -> 0 us
  starting transfers between devices: 7.74 us -> 0 us
  matrix products: 6.9 us -> 0 us
    all_gather x2 -> x0, waiting for transfers between devices: 182 us -> none  [normed_rows(): lax.all_gather(row_block, KV_TP, axis=1, tiled=True).astype(jnp.float32)]
    reduce_scatter x3 -> x0, waiting for transfers between devices: 105 us -> none  [own_block(): tiles = lax.psum_scatter(tiles, axes[k], scatter_dimension=0, tiled=True)]
    pallas_call x0 -> x1, Pallas kernels: none -> 78.5 us  [local(): pl.pallas_call(kernel, out_shape=(jax.ShapeDtypeStruct((32, 128), BF16),...]
    all_to_all x2 -> x0, blocking collectives: 26.9 us -> none  [copy_for_each(): return lax.all_to_all(copies, axis, split_axis=0, concat_axis=0, tiled=True)]
    all_to_all x1 -> x0, waiting for transfers between devices: 11 us -> none  [in_one_piece(): lax.all_to_all(both, axis, split_axis=split_dim, concat_axis=concat_dim,...]
    all_to_all x1 -> x0, starting transfers between devices: 7.54 us -> none  [in_one_piece(): lax.all_to_all(both, axis, split_axis=split_dim, concat_axis=concat_dim,...]
    dot_general x4 -> x0, matrix products: 6.9 us -> none  [the longest x1 3 us: local(): jnp.dot(hidden, down_weight, preferred_element_type=jnp.float32)]
  transfers between devices with their start and end apart: 6 -> 0, of which waited for: 6 -> 0; matrix products, arithmetic and copies ran while one was open for 1% -> 0% of each run, Pallas kernels for 0% -> 0%
where the time goes in v1:
time: 83.5 us; the launch traced here: 82.8 us
  Pallas kernels  78.5 us (94%)
  local copies, waits for them, and re-layouts  3.59 us (4%)
    pallas_call x1, Pallas kernels, local(): pl.pallas_call(kernel, out_shape=(jax.ShapeDtypeStruct((32, 128), BF16),...  78.5 us
    unnamed x2, local copies, waits for them, and re-layouts  3.59 us

profile of v1, /device:TPU:1, one launch (start us, length us, event | category | flops | bytes accessed | tf_op | source)
XLA Modules:
  0.0 82.8 jit_solution(2865142142012660370)
XLA Ops:
  0.6 78.5 %shard_map.140 = (bf16[32,128]{1,0:T(8,128)(2,1)}, f32[2,8,128,128]{3,2,1,0:T(8,128)}) custom-call(bf16[32,128]{1,0:T(8,128)(2,1)} %bitcast.10, f32[32,128]{1,0:T(8,128)} %bitcast.8, bf16[8,2,4096]{2,1,0:T(2,128)(2,1)} %q_h.1, bf16[8,2,4096]{2,1,0:T(2,128)(2,1)} %f_h.1, bf16[8,2,4096]{2,1,0:T(2,128)(2,1)} %v_h.1, bf16[8,2,4096]{2,1,0:T(2,128)(2,1)} %g_h.1, ...), custom_call_target="tpu_custom_call" | custom-call | tf_op jit(solution)/shard_map/pallas_call | solution.py:388
  79.2 1.3 %copy.17 = bf16[128,32]{0,1:T(8,128)(2,1)} copy(bf16[128,32]{0,1:T(8,128)(2,1)} %bitcast.11) | data formatting | bytes 16384
  80.5 2.3 %copy.18 = f32[2,8,128,128]{3,2,1,0:T(8,128)} copy(f32[2,8,128,128]{3,2,1,0:T(8,128)} %get-tuple-element.9) | data formatting | bytes 2097152

commit v2 on v1

--- a/solution.py
+++ b/solution.py
@@ -94,8 +94,8 @@
 
 def kernel(
     x_h, mg_h, q_h, f_h, v_h, g_h, lb_h, st_h, hg_h, ow_h, lg_h, up_h, dn_h,
-    out_ref, nst_h,
-    xv, mg, lg, lb, hg, wraw, upr, dnr, owr, st, nst,
+    out_ref, nst,
+    xv, mg, lg, lb, hg, wraw, upr, dnr, owr, st,
     X, R, D, W2o, W2p, UTs, UTp, DTs, DTp, OWp,
     px1, pr1, px2, pr2, px3, pr3,
     tr, S, B, lbs, msk, O, msg, res, Y, R1, T, R2, wt,
@@ -254,7 +254,6 @@
                 part = act[:, c : c + 1] * new
                 total = part if total is None else total + part
             O[tok, h : h + 1, :] = jnp.sum(total, axis=0, keepdims=True)
-    pltpu.make_async_copy(nst, nst_h, so).start()
     mixed = []
     for tok in range(2):
         o = O[tok]
@@ -378,7 +377,15 @@
     landed(DTp, sd.at[4])
     landed(px2, sd.at[5])
     landed(px3, sd.at[6])
-    pltpu.make_async_copy(nst, nst_h, so).wait()
+
+
+def finish(o_ref, n_ref, out, nst, s0, s1):
+    a = pltpu.make_async_copy(n_ref, nst, s0)
+    b = pltpu.make_async_copy(o_ref, out, s1)
+    a.start()
+    b.start()
+    a.wait()
+    b.wait()
 
 
 def local(tokens, mix_gain, q, f, v, g, lower, state, head_gain, out_w, mlp_gain, up, down):
@@ -389,11 +396,11 @@
         kernel,
         out_shape=(jax.ShapeDtypeStruct((32, 128), BF16), jax.ShapeDtypeStruct(state.shape, F32)),
         in_specs=[pl.BlockSpec(memory_space=pltpu.HBM)] * 13,
-        out_specs=(pl.BlockSpec(memory_space=pltpu.VMEM), pl.BlockSpec(memory_space=pltpu.HBM)),
+        out_specs=(pl.BlockSpec(memory_space=pltpu.VMEM), pl.BlockSpec(memory_space=pltpu.VMEM)),
         scratch_shapes=[
             vm((32, 128), BF16), vm((32, 128), F32), vm((32, 128), F32), vm((8, 128), F32), vm((8, 128), F32),
             vm((64, 4096), BF16), vm((64, 2, 32, 128), BF16), vm((128, 4096), BF16), vm((16, 32, 128), BF16),
-            vm((2, 8, 128, 128), F32), vm((2, 8, 128, 128), F32),
+            vm((2, 8, 128, 128), F32),
             vm((8, 8, 32, 128), BF16), vm((8, 8, 32, 128), BF16), vm((8, 64, 2, 128), BF16),
             vm((8, 2, 64, 128), BF16), vm((8, 2, 64, 128), BF16),
             vm((2, 8, 2, 128, 128), BF16), vm((8, 2, 128, 128), BF16),
@@ -407,11 +414,19 @@
             dma((10,)), *gather_sems, *gather_sems, *gather_sems,
             dma, dma, dma, dma((8,)), dma, dma((8,)), dma((7,)), dma((7,)), dma,
         ],
-        compiler_params=pltpu.CompilerParams(collective_id=0, has_side_effects=True, vmem_limit_bytes=60 * 1024 * 1024),
+        compiler_params=pltpu.CompilerParams(collective_id=0, has_side_effects=True, vmem_limit_bytes=48 * 1024 * 1024),
     )(
-        tokens.T, mix_gain.reshape(32, 128), q, f, v, g, lower, state, head_gain,
+        *(pltpu.with_memory_space_constraint(t, pltpu.HBM) for t in (tokens.T, mix_gain.reshape(32, 128), q, f, v, g, lower, state, head_gain,
         out_w.transpose(0, 2, 1), mlp_gain.reshape(32, 128), up.reshape(64, 2, 32, 128), down,
-    )
+    )))
+    out, nst = pl.pallas_call(
+        finish,
+        out_shape=(jax.ShapeDtypeStruct((32, 128), BF16), jax.ShapeDtypeStruct(state.shape, F32)),
+        in_specs=[pl.BlockSpec(memory_space=pltpu.VMEM)] * 2,
+        out_specs=[pl.BlockSpec(memory_space=pltpu.HBM)] * 2,
+        scratch_shapes=[dma, dma],
+        compiler_params=pltpu.CompilerParams(vmem_limit_bytes=1024*1024),
+    )(out, nst)
     return (out.T, nst)
 
 

time: 83.5 us -> 80.2 us (0.960)
  local copies, waits for them, and re-layouts: 3.59 us -> 0 us
    unnamed x2 -> x0, local copies, waits for them, and re-layouts: 3.59 us -> none
    pallas_call x0 -> x1, Pallas kernels: none -> 0.99 us  [local(): pl.pallas_call(finish, out_shape=(jax.ShapeDtypeStruct((32, 128), BF16),...]
where the time goes in v2:
time: 80.2 us; the launch traced here: 79.6 us
  Pallas kernels  78.9 us (98%)
    pallas_call x1, Pallas kernels, local(): pl.pallas_call(kernel, out_shape=(jax.ShapeDtypeStruct((32, 128), BF16),...  78 us

profile of v2, /device:TPU:1, one launch (start us, length us, event | category | flops | bytes accessed | tf_op | source)
XLA Modules:
  0.0 79.6 jit_solution(4553110505819147792)
XLA Ops:
  0.6 78.0 %shard_map.140 = (bf16[32,128]{1,0:T(8,128)(2,1)S(1)}, f32[2,8,128,128]{3,2,1,0:T(8,128)S(1)}) custom-call(bf16[32,128]{1,0:T(8,128)(2,1)} %bitcast.10, f32[32,128]{1,0:T(8,128)} %bitcast.8, bf16[8,2,4096]{2,1,0:T(2,128)(2,1)} %q_h.1, bf16[8,2,4096]{2,1,0:T(2,128)(2,1)} %f_h.1, bf16[8,2,4096]{2,1,0:T(2,128)(2,1)} %v_h.1, bf16[8,2,4096]{2,1,0:T(2,128)(2,1)} %g_h.1, ...), custom_call_target="tpu_custom_call" | custom-call | tf_op jit(solution)/shard_map/pallas_call | solution.py:395
  78.6 1.0 %shard_map.141 = (bf16[32,128]{1,0:T(8,128)(2,1)}, f32[2,8,128,128]{3,2,1,0:T(8,128)}) custom-call(bf16[32,128]{1,0:T(8,128)(2,1)S(1)} %get-tuple-element.6.o_ref, f32[2,8,128,128]{3,2,1,0:T(8,128)S(1)} %get-tuple-element.7.n_ref), custom_call_target="tpu_custom_call" | custom-call | tf_op jit(solution)/shard_map/pallas_call | solution.py:422
